TPU v7x, 32 devices: a whole 2x2x4 slice. The times are simulated.
32 devices in a mesh: kv: 8 (over z, x), tp: 4 (over y, core).
Axes of the slice: x: 2, y: 2, z: 4, core: 2. Of those that a mesh axis runs over, the one named last changes fastest.
Arguments:
- tokens: bfloat16 [384, 4096], P(None, ('kv', 'tp')), may hold values from -90 to 90
- norm_gain: float32 [4096], P('kv'), may hold values from 0.1 to 1.9
- w_query: bfloat16 [4096, 2048], P('kv', 'tp'), may hold values from -0.09375 to 0.09375
- w_key: bfloat16 [4096, 2048], P('kv', 'tp'), may hold values from -0.09375 to 0.09375
- w_value: bfloat16 [4096, 2048], P('kv', 'tp'), may hold values from -0.09375 to 0.09375
- w_outgate: bfloat16 [4096, 2048], P('kv', 'tp'), may hold values from -0.09375 to 0.09375
- w_igate: bfloat16 [4096, 16], replicated, may hold values from -0.09375 to 0.09375
- w_fgate: bfloat16 [4096, 16], replicated, may hold values from -0.09375 to 0.09375
- forget_bias: float32 [16], P('tp'), may hold values from -1 to 5
- head_gain: float32 [2048], P('tp'), may hold values from 0.1 to 1.9
- w_proj: bfloat16 [2048, 4096], P('tp', 'kv'), may hold values from -0.125 to 0.125
- mixer_gain: float32 [4096], P('kv'), may hold values from 0.1 to 1.9
- w_gate: bfloat16 [4096, 11264], P('kv', 'tp'), may hold values from -0.09375 to 0.09375
- w_up: bfloat16 [4096, 11264], P('kv', 'tp'), may hold values from -0.09375 to 0.09375
- w_down: bfloat16 [11264, 4096], P('tp', 'kv'), may hold values from -0.0546875 to 0.0546875
- state_c: float32 [384, 16, 128, 128], P('kv', 'tp'), may hold values from -0.5 to 0.5
- state_m: float32 [384, 16], P('kv', 'tp'), may hold values from -4 to 4
- tail_keys: bfloat16 [384, 16, 64, 128], P('kv', 'tp'), may hold values from -6 to 6
- tail_values: bfloat16 [384, 16, 64, 128], P('kv', 'tp'), may hold values from -6 to 6
- tail_gate: float32 [384, 16, 64], P('kv', 'tp'), may hold values from -8 to 130
- block_forget: float32 [384, 16], P('kv', 'tp'), may hold values from -6 to 0
- lengths: int32 [384], P('kv'), may hold values from 1 to 64, 6144 in all
Outputs:
- result: bfloat16 [384, 4096], P(None, ('kv', 'tp'))
All inputs are finite; a program needn't handle non-finite values. No bound on the sum of `lengths` on one device may be relied on, other than what follows from the above.
Results may differ from a plain program's by a relative error of at most 0.012.
Values may be sent and summed in bfloat16 or wider, within the bound.
A program may use at most 128 MiB of HBM per device.

v0:
```python
import jax
import jax.numpy as jnp
from jax import lax
from jax.sharding import PartitionSpec as P

D = 4096
EPS = 1e-06


def recall(
    query,
    key,
    value,
    igate,
    fpre,
    state_c,
    state_m,
    tail_keys,
    tail_values,
    tail_gate,
    block_forget,
    lengths,
):
    f32 = jnp.float32
    span = tail_keys.shape[2]
    head_dim = query.shape[2]
    running = block_forget + jax.nn.log_sigmoid(fpre)
    inter = running + state_m
    live = jnp.arange(span, dtype=jnp.int32)[None, :] < lengths[:, None]
    tail_log = jnp.where(live[:, None, :], running[:, :, None] + tail_gate, -jnp.inf)
    top = jnp.maximum(jnp.maximum(inter, jnp.max(tail_log, axis=2)), igate)
    w_inter = jnp.exp(inter - top)
    w_tail = jnp.exp(tail_log - top[:, :, None])
    w_own = jnp.exp(igate - top)
    scores = jnp.einsum("shpd,shd->shp", tail_keys.astype(f32), query) * head_dim ** (-0.5)
    own = jnp.sum(query * key, axis=2)
    memory = jnp.einsum("shvk,shk->shv", state_c, query)
    weighted = w_tail * scores
    return (
        w_inter[:, :, None] * memory
        + jnp.einsum("shp,shpv->shv", weighted, tail_values.astype(f32))
        + (w_own * own)[:, :, None] * value
    )


def per_device(
    tokens,
    norm_gain,
    w_query,
    w_key,
    w_value,
    w_outgate,
    w_igate,
    w_fgate,
    forget_bias,
    head_gain,
    w_proj,
    mixer_gain,
    w_gate,
    w_up,
    w_down,
    state_c,
    state_m,
    tail_keys,
    tail_values,
    tail_gate,
    block_forget,
    lengths,
):
    f32 = jnp.float32
    bf = jnp.bfloat16
    kv_pos = lax.axis_index("kv")
    tp_pos = lax.axis_index("tp")
    rows = norm_gain.shape[0]
    heads = forget_bias.shape[0]
    head_dim = tail_keys.shape[3]
    seq_dev = lengths.shape[0]
    width = heads * head_dim
    wide = lax.all_gather(tokens, "tp", axis=1, tiled=True)
    widef = wide.astype(f32)
    scaled = (widef * norm_gain).astype(bf)

    def local_cols(weight):
        return lax.dynamic_slice(weight, (kv_pos * rows, tp_pos * heads), (rows, heads))

    gate_weights = jnp.concatenate([local_cols(w_igate), local_cols(w_fgate)], axis=1)
    joined = jnp.concatenate([w_query, w_key, w_value, w_outgate], axis=1)
    proj = jnp.dot(scaled, joined, preferred_element_type=f32)
    gates = jnp.dot(scaled, gate_weights, preferred_element_type=f32)
    tokf = tokens.astype(f32)
    sq_all = lax.psum(jnp.sum(tokf * tokf, axis=1), ("kv", "tp"))
    proj, gates = (
        lax.psum_scatter(proj, "kv", scatter_dimension=0, tiled=True),
        lax.psum_scatter(gates, "kv", scatter_dimension=0, tiled=True),
    )
    inv_first = lax.dynamic_slice_in_dim(lax.rsqrt(sq_all / D + EPS), kv_pos * seq_dev, seq_dev)
    proj = proj * inv_first[:, None]
    gates = gates * inv_first[:, None]
    query = proj[:, :width].reshape(seq_dev, heads, head_dim)
    key = proj[:, width : 2 * width].reshape(seq_dev, heads, head_dim) * head_dim ** (-0.5)
    value = proj[:, 2 * width : 3 * width].reshape(seq_dev, heads, head_dim)
    outgate = proj[:, 3 * width :]
    igate = gates[:, :heads]
    fpre = gates[:, heads:] + forget_bias
    recalled = recall(
        query,
        key,
        value,
        igate,
        fpre,
        state_c,
        state_m,
        tail_keys,
        tail_values,
        tail_gate,
        block_forget,
        lengths,
    )
    normed = recalled * lax.rsqrt(jnp.mean(recalled * recalled, axis=2, keepdims=True) + EPS)
    mixed = (normed.reshape(seq_dev, width) * head_gain * jax.nn.sigmoid(outgate)).astype(bf)
    partial_value = jnp.dot(
        lax.all_gather(mixed, "kv", axis=0, tiled=True), w_proj, preferred_element_type=f32
    )
    attended = lax.psum(partial_value.astype(jnp.bfloat16), "tp").astype(jnp.float32)
    middle = (widef + attended).astype(bf)
    middlef = middle.astype(f32)
    part_sq2 = jnp.sum(middlef * middlef, axis=1)
    scaled_mid = (middlef * mixer_gain).astype(bf)
    gate_part = jnp.dot(scaled_mid, w_gate, preferred_element_type=f32)
    up_part = jnp.dot(scaled_mid, w_up, preferred_element_type=f32)
    gate_sh, up_sh, sq_sh = (
        lax.psum_scatter(gate_part, "kv", scatter_dimension=0, tiled=True),
        lax.psum_scatter(up_part, "kv", scatter_dimension=0, tiled=True),
        lax.psum_scatter(part_sq2, "kv", scatter_dimension=0, tiled=True),
    )
    inv_second = lax.rsqrt(sq_sh / D + EPS)[:, None]
    hidden_sh = (jax.nn.silu(gate_sh * inv_second) * (up_sh * inv_second)).astype(bf)
    down_part = jnp.dot(
        lax.all_gather(hidden_sh, "kv", axis=0, tiled=True), w_down, preferred_element_type=f32
    )
    down_sum = lax.psum_scatter(
        down_part.astype(jnp.bfloat16), "tp", scatter_dimension=1, tiled=True
    ).astype(jnp.float32)
    columns = down_sum.shape[1]
    residual = lax.dynamic_slice_in_dim(middlef, tp_pos * columns, columns, 1)
    return (residual + down_sum).astype(bf)


def solution(mesh):
    return jax.shard_map(
        per_device,
        mesh=mesh,
        in_specs=(
            P(None, ("kv", "tp")),
            P("kv"),
            P("kv", "tp"),
            P("kv", "tp"),
            P("kv", "tp"),
            P("kv", "tp"),
            P(),
            P(),
            P("tp"),
            P("tp"),
            P("tp", "kv"),
            P("kv"),
            P("kv", "tp"),
            P("kv", "tp"),
            P("tp", "kv"),
            P("kv", "tp", None, None),
            P("kv", "tp"),
            P("kv", "tp", None, None),
            P("kv", "tp", None, None),
            P("kv", "tp", None),
            P("kv", "tp"),
            P("kv"),
        ),
        out_specs=P(None, ("kv", "tp")),
        check_vma=False,
    )
```

profile of v0, /device:TPU:0, one launch (start us, length us, event | category | flops | bytes accessed | tf_op | source)
XLA Modules:
  0.0 528.5 jit_solution(12030437930786760978)
XLA Ops:
  8.3 8.2 %all_gather.9 = bf16[384,512]{1,0:T(8,128)(2,1)S(1)} all-gather(bf16[384,128]{1,0:T(8,128)(2,1)} %param.22), channel_id=1, replica_groups=mesh['kv'=8,'tp'=4] {'tp'}, dimensions={1}, use_global_device_ids=true | all-gather | bytes 491520 | tf_op jit(solution)/shard_map/all_gather | solution.py:79
  16.5 1.6 fusion.12
  18.1 4.2 fusion
  23.4 40.2 %psum.14 = f32[384]{0:T(512)S(1)} all-reduce(f32[384]{0:T(512)S(1)} %multiply_reduce_fusion.1), channel_id=1, replica_groups=mesh['kv'=8,'tp'=4] {'kv','tp'}, use_global_device_ids=true, to_apply=%region_2.0 | all-reduce | flops 384 | bytes 3072 | tf_op jit(solution)/shard_map/psum | solution.py:91
  64.3 16.8 %reduce-scatter.16.cloned.1.call-done = f32[48,8]{1,0:T(8,128)} async-done(((f32[384,8]{1,0:T(8,128)}), f32[48,8]{1,0:T(8,128)}) %reduce-scatter.16.cloned.1.call-update) | async-done | bytes 1552
  82.5 1.4 fusion.33
  84.5 1.7 fusion.21
  86.2 1.4 copy.38
  89.6 1.4 copy.39
  91.0 67.4 %reduce-scatter.10.cloned.1.call-done = f32[48,2048]{1,0:T(8,128)} async-done(((f32[384,2048]{1,0:T(8,128)}), f32[48,2048]{1,0:T(8,128)}) %reduce-scatter.10.cloned.1.call-update) | async-done | bytes 393232 | tf_op jit(solution)/shard_map/reduce_scatter | solution.py:93
  160.9 1.6 reshape.50
  162.5 1.5 reshape.47
  164.0 1.6 mul.152
  165.6 1.7 multiply_reduce_fusion.3
  167.3 1.4 copy.41
  169.9 1.4 copy.42
  171.3 4.3 fusion.36
  175.7 8.6 %fusion.35 = f32[48,4,1,128]{3,2,1,0:T(1,128)} fusion(f32[48,4,128,1]{2,3,1,0:T(1,128)S(1)} %bitcast.36, f32[48,4,128,128]{3,2,1,0:T(8,128)} %param.37), kind=kOutput, calls=%fused_computation.58 | convolution fusion | flops 6291456 | bytes 12779520 | tf_op jit(solution)/shard_map/shvk,shk->shv/dot_general | solution.py:37
  184.2 1.6 reshape.48
  189.3 31.0 %all_gather.10 = bf16[384,512]{1,0:T(8,128)(2,1)S(1)} all-gather(bf16[48,512]{1,0:T(8,128)(2,1)S(1)} %fusion.17), channel_id=1, replica_groups=mesh['kv'=8,'tp'=4] {'kv'}, dimensions={0}, use_global_device_ids=true | all-gather | bytes 442368 | tf_op jit(solution)/shard_map/all_gather | solution.py:122
  221.5 32.0 %all-reduce.3.cloned.1.call-done = bf16[384,512]{1,0:T(8,128)(2,1)} async-done(((bf16[384,512]{1,0:T(8,128)(2,1)}), bf16[384,512]{1,0:T(8,128)(2,1)}) %all-reduce.3.cloned.1.call-update) | async-done | bytes 393232 | tf_op jit(solution)/shard_map/psum | solution.py:124
  253.5 5.2 fusion.15
  258.8 5.3 fusion.14
  265.9 2.1 fusion.10
  268.0 22.5 %all-reduce = f32[384]{0:T(512)S(1)} all-reduce(f32[384]{0:T(512)S(1)} %get-tuple-element.12), channel_id=5, replica_groups=mesh['kv'=8,'tp'=4] {'kv'}, use_global_device_ids=true, to_apply=%region_10.11.clone | all-reduce | flops 384 | bytes 3072
  290.6 59.3 %reduce-scatter.12.cloned.1.call-done = f32[48,2816]{1,0:T(8,128)} async-done(((f32[384,2816]{1,0:T(8,128)}), f32[48,2816]{1,0:T(8,128)}) %reduce-scatter.12.cloned.1.call-update) | async-done | bytes 540688 | tf_op jit(solution)/shard_map/reduce_scatter | solution.py:132
  349.8 93.3 %reduce-scatter.14.cloned.1.call-done = f32[48,2816]{1,0:T(8,128)} async-done(((f32[384,2816]{1,0:T(8,128)}), f32[48,2816]{1,0:T(8,128)}) %reduce-scatter.14.cloned.1.call-update) | async-done | bytes 540688 | tf_op jit(solution)/shard_map/reduce_scatter | solution.py:133
  443.1 2.2 multiply_convert_fusion.1
  445.4 49.5 %all-gather.2.cloned.1.call-done = bf16[384,2816]{1,0:T(8,128)(2,1)} async-done(((bf16[48,2816]{1,0:T(8,128)(2,1)}), bf16[384,2816]{1,0:T(8,128)(2,1)}) %all-gather.2.cloned.1.call-update) | async-done | bytes 2162704 | tf_op jit(solution)/shard_map/all_gather | solution.py:139
  494.9 3.7 convolution_convert_fusion
  499.6 19.5 %reduce-scatter.18.cloned.1.call-done = bf16[128,384]{1,0:T(8,128)(2,1)} async-done(((bf16[512,384]{1,0:T(8,128)(2,1)}), bf16[128,384]{1,0:T(8,128)(2,1)}) %reduce-scatter.18.cloned.1.call-update) | async-done | bytes 98320
  520.1 1.6 add_convert_fusion
  (63 shorter events, 19.3 us)
Async XLA Ops:
  6.5 180.5 %copy-start = (bf16[48,4,64,128]{3,2,1,0:T(8,128)(2,1)S(1)}, bf16[48,4,64,128]{3,2,1,0:T(8,128)(2,1)}, u32[]{:S(2)}) copy-start(bf16[48,4,64,128]{3,2,1,0:T(8,128)(2,1)} %param.40) | copy-start | bytes 9437188
  6.5 74.6 %reduce-scatter.16.cloned.1.call-start = ((), (), s32[]{:S(2)}) async-start(), calls=%async_computation.10 | async-start | bytes 221184
  18.1 140.3 %reduce-scatter.10.cloned.1.call-start = ((), (), s32[]{:S(2)}) async-start(), calls=%async_computation.5 | async-start | bytes 3538944 | tf_op jit(solution)/shard_map/reduce_scatter | solution.py:93
  22.3 41.9 %copy-start.10 = (s32[48]{0:T(128)S(1)}, s32[48]{0:T(128)}, u32[]{:S(2)}) copy-start(s32[48]{0:T(128)} %param.43) | copy-start | bytes 580
  22.3 231.1 %all-reduce.3.cloned.1.call-start = ((), (), s32[]{:S(2)}) async-start(), calls=%async_computation.6 | async-start | bytes 786432 | tf_op jit(solution)/shard_map/psum | solution.py:124
  159.5 0.7 copy-start.1
  171.3 4.3 copy-start.4
  184.2 4.2 copy-start.9
  185.8 2.2 copy-start.3
  185.8 2.2 copy-start.5
  185.8 2.2 copy-start.6
  185.8 2.2 copy-start.7
  185.8 34.5 %copy-start.2 = (bf16[512,512]{1,0:T(8,128)(2,1)S(1)}, bf16[512,512]{1,0:T(8,128)(2,1)}, u32[]{:S(2)}) copy-start(bf16[512,512]{1,0:T(8,128)(2,1)} %param.32) | copy-start | bytes 1572868
  187.0 66.4 %copy-start.8 = (f32[512]{0:T(512)S(1)}, f32[512]{0:T(512)}, u32[]{:S(2)}) copy-start(f32[512]{0:T(512)} %param.33) | copy-start | bytes 6148
  221.4 128.4 %reduce-scatter.12.cloned.1.call-start = ((), (), s32[]{:S(2)}) async-start(), calls=%async_computation.7 | async-start | bytes 4866048 | tf_op jit(solution)/shard_map/reduce_scatter | solution.py:132
  258.7 184.4 %reduce-scatter.14.cloned.1.call-start = ((), (), s32[]{:S(2)}) async-start(), calls=%async_computation.8 | async-start | bytes 4866048 | tf_op jit(solution)/shard_map/reduce_scatter | solution.py:133
  264.0 0.7 copy-start.11
  264.0 230.9 %all-gather.2.cloned.1.call-start = ((), (), s32[]{:S(2)}) async-start(), calls=%async_computation.9 | async-start | bytes 2433024 | tf_op jit(solution)/shard_map/all_gather | solution.py:139
  445.3 73.8 %reduce-scatter.18.cloned.1.call-start = ((), (), s32[]{:S(2)}) async-start(), calls=%async_computation.11 | async-start | bytes 491520
Sparse Core Ops, SparseCore 0:
  18.2 62.8 reduce-scatter.15
  84.7 73.6 reduce-scatter.9
  221.6 31.8 all-reduce.2
  258.8 90.9 reduce-scatter.11
  353.3 89.8 reduce-scatter.13
  445.5 49.4 all-gather.1
  499.7 19.3 reduce-scatter.17
where the time goes:
time: 530 us; the launch traced here: 529 us
  waiting for transfers between devices  338 us (64%)
  blocking collectives  102 us (19%)
  matrix products  34.9 us (7%)
  local copies, waits for them, and re-layouts  20.1 us (4%)
  other arithmetic  19.2 us (4%)
  between operations  14.3 us (3%)
    reduce_scatter x1, waiting for transfers between devices, per_device(): lax.psum_scatter(up_part, 'kv', scatter_dimension=0, tiled=True)  93.3 us
    reduce_scatter x1, waiting for transfers between devices, per_device(): lax.psum_scatter(proj, 'kv', scatter_dimension=0, tiled=True)  67.4 us
    reduce_scatter x1, waiting for transfers between devices, per_device(): lax.psum_scatter(gate_part, 'kv', scatter_dimension=0, tiled=True)  59.3 us
    all_gather x1, waiting for transfers between devices, per_device(): lax.all_gather(hidden_sh, 'kv', axis=0, tiled=True)  49.5 us
    psum x1, blocking collectives, per_device(): sq_all = lax.psum(jnp.sum(tokf * tokf, axis=1), ('kv', 'tp'))  40.2 us
    unnamed x9, waiting for transfers between devices  36.4 us
    psum x1, waiting for transfers between devices, per_device(): lax.psum(partial_value.astype(jnp.bfloat16), 'tp').astype(jnp.float32)  32 us
    all_gather x1, blocking collectives, per_device(): lax.all_gather(mixed, 'kv', axis=0, tiled=True)  31 us
  transfers between devices with their start and end apart: 7, of which 7 were waited for; matrix products, arithmetic and copies ran while one was open for 4% of the time, Pallas kernels for 0%

commit v1 on v0

--- a/solution.py
+++ b/solution.py
@@ -5,6 +5,11 @@
 
 D = 4096
 EPS = 1e-06
+
+
+def exchange_gather(x, axis, along):
+    stack = jnp.stack([x] * lax.axis_size(axis))
+    return jnp.concatenate(lax.all_to_all(stack, axis, 0, 0), axis=along)
 
 
 def recall(
@@ -118,9 +123,7 @@
     )
     normed = recalled * lax.rsqrt(jnp.mean(recalled * recalled, axis=2, keepdims=True) + EPS)
     mixed = (normed.reshape(seq_dev, width) * head_gain * jax.nn.sigmoid(outgate)).astype(bf)
-    partial_value = jnp.dot(
-        lax.all_gather(mixed, "kv", axis=0, tiled=True), w_proj, preferred_element_type=f32
-    )
+    partial_value = jnp.dot(exchange_gather(mixed, "kv", 0), w_proj, preferred_element_type=f32)
     attended = lax.psum(partial_value.astype(jnp.bfloat16), "tp").astype(jnp.float32)
     middle = (widef + attended).astype(bf)
     middlef = middle.astype(f32)

time: 530 us -> 514 us (0.970)
  blocking collectives: 102 us -> 86.1 us
    all_gather x1 -> x0, blocking collectives: 31 us -> none  [per_device(): lax.all_gather(mixed, 'kv', axis=0, tiled=True)]
    all_to_all x0 -> x1, blocking collectives: none -> 15.3 us  [exchange_gather(): return jnp.concatenate(lax.all_to_all(stack, axis, 0, 0), axis=along)]
  transfers between devices with their start and end apart: 7 -> 7, of which waited for: 7 -> 7; matrix products, arithmetic and copies ran while one was open for 4% -> 5% of each run, Pallas kernels for 0% -> 0%
where the time goes in v1:
time: 514 us; the launch traced here: 512 us
  waiting for transfers between devices  337 us (66%)
  blocking collectives  86.1 us (17%)
  matrix products  34.9 us (7%)
  local copies, waits for them, and re-layouts  20.1 us (4%)
  other arithmetic  19.2 us (4%)
  between operations  14.3 us (3%)
    reduce_scatter x1, waiting for transfers between devices, per_device(): lax.psum_scatter(up_part, 'kv', scatter_dimension=0, tiled=True)  93.3 us
    reduce_scatter x1, waiting for transfers between devices, per_device(): lax.psum_scatter(proj, 'kv', scatter_dimension=0, tiled=True)  67.4 us
    reduce_scatter x1, waiting for transfers between devices, per_device(): lax.psum_scatter(gate_part, 'kv', scatter_dimension=0, tiled=True)  59.3 us
    all_gather x1, waiting for transfers between devices, per_device(): lax.all_gather(hidden_sh, 'kv', axis=0, tiled=True)  49.5 us
    psum x1, blocking collectives, per_device(): sq_all = lax.psum(jnp.sum(tokf * tokf, axis=1), ('kv', 'tp'))  40.2 us
    unnamed x9, waiting for transfers between devices  36.4 us
    psum x1, waiting for transfers between devices, per_device(): lax.psum(partial_value.astype(jnp.bfloat16), 'tp').astype(jnp.float32)  31.5 us
    unnamed x1, blocking collectives  22.4 us
  transfers between devices with their start and end apart: 7, of which 7 were waited for; matrix products, arithmetic and copies ran while one was open for 5% of the time, Pallas kernels for 0%

profile of v1, /device:TPU:0, one launch (start us, length us, event | category | flops | bytes accessed | tf_op | source)
XLA Modules:
  0.0 512.4 jit_solution(15412349482084126812)
XLA Ops:
  8.3 8.2 %all_gather.6 = bf16[384,512]{1,0:T(8,128)(2,1)S(1)} all-gather(bf16[384,128]{1,0:T(8,128)(2,1)} %param.22), channel_id=1, replica_groups=mesh['kv'=8,'tp'=4] {'tp'}, dimensions={1}, use_global_device_ids=true | all-gather | bytes 491520 | tf_op jit(solution)/shard_map/all_gather | solution.py:84
  16.5 1.6 fusion.12
  18.1 4.2 fusion
  23.4 40.2 %psum.14 = f32[384]{0:T(512)S(1)} all-reduce(f32[384]{0:T(512)S(1)} %multiply_reduce_fusion.1), channel_id=1, replica_groups=mesh['kv'=8,'tp'=4] {'kv','tp'}, use_global_device_ids=true, to_apply=%region_2.0 | all-reduce | flops 384 | bytes 3072 | tf_op jit(solution)/shard_map/psum | solution.py:96
  64.3 16.8 %reduce-scatter.16.cloned.1.call-done = f32[48,8]{1,0:T(8,128)} async-done(((f32[384,8]{1,0:T(8,128)}), f32[48,8]{1,0:T(8,128)}) %reduce-scatter.16.cloned.1.call-update) | async-done | bytes 1552
  82.5 1.4 fusion.33
  84.5 1.7 fusion.21
  86.2 1.4 copy.38
  89.6 1.4 copy.39
  91.0 67.4 %reduce-scatter.10.cloned.1.call-done = f32[48,2048]{1,0:T(8,128)} async-done(((f32[384,2048]{1,0:T(8,128)}), f32[48,2048]{1,0:T(8,128)}) %reduce-scatter.10.cloned.1.call-update) | async-done | bytes 393232 | tf_op jit(solution)/shard_map/reduce_scatter | solution.py:98
  160.9 1.6 reshape.56
  162.5 1.5 reshape.52
  164.0 1.6 mul.152
  165.6 1.7 multiply_reduce_fusion.3
  167.3 1.4 copy.41
  169.9 1.4 copy.42
  171.3 4.3 fusion.36
  175.7 8.6 %fusion.35 = f32[48,4,1,128]{3,2,1,0:T(1,128)} fusion(f32[48,4,128,1]{2,3,1,0:T(1,128)S(1)} %bitcast.38, f32[48,4,128,128]{3,2,1,0:T(8,128)} %param.37), kind=kOutput, calls=%fused_computation.58 | convolution fusion | flops 6291456 | bytes 12779520 | tf_op jit(solution)/shard_map/shvk,shk->shv/dot_general | solution.py:42
  184.2 1.6 reshape.53
  189.3 15.3 %all_to_all.5 = bf16[8,48,512]{2,1,0:T(8,128)(2,1)S(1)} all-to-all(bf16[8,48,512]{2,1,0:T(8,128)(2,1)S(1)} %stack.2), channel_id=1, replica_groups=mesh['kv'=8,'tp'=4] {'kv'}, dimensions={0} | all-to-all | bytes 786432 | tf_op jit(solution)/shard_map/all_to_all | solution.py:12
  205.8 31.5 %all-reduce.3.cloned.1.call-done = bf16[384,512]{1,0:T(8,128)(2,1)} async-done(((bf16[384,512]{1,0:T(8,128)(2,1)}), bf16[384,512]{1,0:T(8,128)(2,1)}) %all-reduce.3.cloned.1.call-update) | async-done | bytes 393232 | tf_op jit(solution)/shard_map/psum | solution.py:127
  237.4 5.2 %fusion.15 = f32[384,2816]{1,0:T(8,128)} fusion(bf16[512,2816]{1,0:T(8,128)(2,1)} %param.34, f32[512]{0:T(512)S(1)} %copy-done.8, bf16[384,512]{1,0:T(8,128)(2,1)} %all-reduce.3.cloned.1.call-done, bf16[384,512]{1,0:T(8,128)(2,1)S(1)} %all_gather.6), kind=kOutput, calls=%fused_computation.23 | convolution fusion | flops 1108672512 | bytes 7997440 | tf_op jit(solution)/shard_map/dot_general | solution.py:132
  242.7 5.3 %fusion.14 = f32[384,2816]{1,0:T(8,128)} fusion(bf16[512,2816]{1,0:T(8,128)(2,1)} %param.35, f32[512]{0:T(512)S(1)} %copy-done.8, bf16[384,512]{1,0:T(8,128)(2,1)} %all-reduce.3.cloned.1.call-done, bf16[384,512]{1,0:T(8,128)(2,1)S(1)} %all_gather.6), kind=kOutput, calls=%fused_computation.22 | convolution fusion | flops 1108672512 | bytes 7997440 | tf_op jit(solution)/shard_map/dot_general | solution.py:133
  249.8 2.1 fusion.10
  251.9 22.4 %all-reduce = f32[384]{0:T(512)S(1)} all-reduce(f32[384]{0:T(512)S(1)} %get-tuple-element.12), channel_id=5, replica_groups=mesh['kv'=8,'tp'=4] {'kv'}, use_global_device_ids=true, to_apply=%region_10.11.clone | all-reduce | flops 384 | bytes 3072
  274.5 59.3 %reduce-scatter.12.cloned.1.call-done = f32[48,2816]{1,0:T(8,128)} async-done(((f32[384,2816]{1,0:T(8,128)}), f32[48,2816]{1,0:T(8,128)}) %reduce-scatter.12.cloned.1.call-update) | async-done | bytes 540688 | tf_op jit(solution)/shard_map/reduce_scatter | solution.py:135
  333.7 93.3 %reduce-scatter.14.cloned.1.call-done = f32[48,2816]{1,0:T(8,128)} async-done(((f32[384,2816]{1,0:T(8,128)}), f32[48,2816]{1,0:T(8,128)}) %reduce-scatter.14.cloned.1.call-update) | async-done | bytes 540688 | tf_op jit(solution)/shard_map/reduce_scatter | solution.py:136
  427.0 2.2 multiply_convert_fusion.1
  429.3 49.5 %all-gather.2.cloned.1.call-done = bf16[384,2816]{1,0:T(8,128)(2,1)} async-done(((bf16[48,2816]{1,0:T(8,128)(2,1)}), bf16[384,2816]{1,0:T(8,128)(2,1)}) %all-gather.2.cloned.1.call-update) | async-done | bytes 2162704 | tf_op jit(solution)/shard_map/all_gather | solution.py:142
  478.8 3.7 convolution_convert_fusion
  483.5 19.5 %reduce-scatter.18.cloned.1.call-done = bf16[128,384]{1,0:T(8,128)(2,1)} async-done(((bf16[512,384]{1,0:T(8,128)(2,1)}), bf16[128,384]{1,0:T(8,128)(2,1)}) %reduce-scatter.18.cloned.1.call-update) | async-done | bytes 98320
  504.0 1.6 add_convert_fusion
  (64 shorter events, 19.4 us)
Async XLA Ops:
  6.5 180.5 %copy-start = (bf16[48,4,64,128]{3,2,1,0:T(8,128)(2,1)S(1)}, bf16[48,4,64,128]{3,2,1,0:T(8,128)(2,1)}, u32[]{:S(2)}) copy-start(bf16[48,4,64,128]{3,2,1,0:T(8,128)(2,1)} %param.40) | copy-start | bytes 9437188
  6.5 74.6 %reduce-scatter.16.cloned.1.call-start = ((), (), s32[]{:S(2)}) async-start(), calls=%async_computation.11 | async-start | bytes 221184
  18.1 140.3 %reduce-scatter.10.cloned.1.call-start = ((), (), s32[]{:S(2)}) async-start(), calls=%async_computation.6 | async-start | bytes 3538944 | tf_op jit(solution)/shard_map/reduce_scatter | solution.py:98
  22.3 41.9 %copy-start.10 = (s32[48]{0:T(128)S(1)}, s32[48]{0:T(128)}, u32[]{:S(2)}) copy-start(s32[48]{0:T(128)} %param.43) | copy-start | bytes 580
  22.3 215.0 %all-reduce.3.cloned.1.call-start = ((), (), s32[]{:S(2)}) async-start(), calls=%async_computation.7 | async-start | bytes 786432 | tf_op jit(solution)/shard_map/psum | solution.py:127
  159.5 0.7 copy-start.1
  171.3 4.3 copy-start.4
  184.2 4.2 copy-start.9
  185.8 2.2 copy-start.3
  185.8 2.2 copy-start.5
  185.8 2.2 copy-start.6
  185.8 2.2 copy-start.7
  185.8 18.9 %copy-start.2 = (bf16[512,512]{1,0:T(8,128)(2,1)S(1)}, bf16[512,512]{1,0:T(8,128)(2,1)}, u32[]{:S(2)}) copy-start(bf16[512,512]{1,0:T(8,128)(2,1)} %param.32) | copy-start | bytes 1572868
  187.0 50.4 %copy-start.8 = (f32[512]{0:T(512)S(1)}, f32[512]{0:T(512)}, u32[]{:S(2)}) copy-start(f32[512]{0:T(512)} %param.33) | copy-start | bytes 6148
  205.8 127.9 %reduce-scatter.12.cloned.1.call-start = ((), (), s32[]{:S(2)}) async-start(), calls=%async_computation.8 | async-start | bytes 4866048 | tf_op jit(solution)/shard_map/reduce_scatter | solution.py:135
  242.6 184.4 %reduce-scatter.14.cloned.1.call-start = ((), (), s32[]{:S(2)}) async-start(), calls=%async_computation.9 | async-start | bytes 4866048 | tf_op jit(solution)/shard_map/reduce_scatter | solution.py:136
  247.9 0.7 copy-start.11
  248.0 230.8 %all-gather.2.cloned.1.call-start = ((), (), s32[]{:S(2)}) async-start(), calls=%async_computation.10 | async-start | bytes 2433024 | tf_op jit(solution)/shard_map/all_gather | solution.py:142
  429.2 73.8 %reduce-scatter.18.cloned.1.call-start = ((), (), s32[]{:S(2)}) async-start(), calls=%async_computation.12 | async-start | bytes 491520
Sparse Core Ops, SparseCore 0:
  18.2 62.8 reduce-scatter.15
  84.7 73.6 reduce-scatter.9
  205.9 31.4 all-reduce.2
  242.8 90.9 reduce-scatter.11
  337.2 89.8 reduce-scatter.13
  429.3 49.4 all-gather.1
  483.6 19.3 reduce-scatter.17
